TPU v7x, 32 devices: a whole 2x2x4 slice. The times are simulated.
32 devices in a mesh: fs: 4 (over y, x), tp: 8 (over z, core).
Axes of the slice: x: 2, y: 2, z: 4, core: 2. Of those that a mesh axis runs over, the one named last changes fastest.
Arguments:
- saved_inputs: bfloat16 [2688, 4096], P('fs', 'tp'), may hold values from -6 to 6
- proj_cotangent: bfloat16 [2688, 4096], P('fs', 'tp'), may hold values from -0.115722656 to 0.115722656
- saved_hidden: bfloat16 [2688, 4096], P('fs', 'tp'), may hold values from -6 to 6
- out_cotangent: bfloat16 [2688, 4096], P('fs', 'tp'), may hold values from -0.115722656 to 0.115722656
- factors: bfloat16 [2, 4096, 128], replicated, may hold values from -0.46875 to 0.46875
- w_proj: float32 [4096, 4096], P('fs', 'tp'), may hold values from -0.09375 to 0.09375
- w_out: float32 [4096, 4096], P('tp', 'fs'), may hold values from -0.09375 to 0.09375
- moment_first: float32 [2, 128, 4096], P(None, None, 'tp'), may hold values from -1.8 to 1.8
- moment_second: float32 [2, 128, 4096], P(None, None, 'tp'), may hold values from 0.05 to 1
Outputs:
- proj_next: float32 [4096, 4096], P('fs', 'tp')
- out_next: float32 [4096, 4096], P('tp', 'fs')
- proj_copy: bfloat16 [4096, 4096], P(None, 'tp')
- out_copy: bfloat16 [4096, 4096], P('tp')
- first_next: float32 [2, 128, 4096], P(None, None, 'tp')
- second_next: float32 [2, 128, 4096], P(None, None, 'tp')
All inputs are finite; a program needn't handle non-finite values.
Results may differ from a plain program's by a relative error of at most 0.001.
Values may be sent and summed in bfloat16 or wider, within the bound.
A program may use at most 64 MiB of HBM per device.

v0:
```python
import jax
import jax.numpy as jnp
from jax import lax
from jax.sharding import PartitionSpec as P

beta_first = 0.9
beta_second = 0.95
learn_rate = 0.02
epsilon = 1e-06


def over_tokens(left_rows, right_rows, precise):
    return lax.dot_general(
        left_rows,
        right_rows,
        (((0,), (0,)), ((), ())),
        preferred_element_type=jnp.float32,
        precision=precise,
    )


def body(
    saved_inputs,
    proj_cotangent,
    saved_hidden,
    out_cotangent,
    factors,
    w_proj,
    w_out,
    moment_first,
    moment_second,
):
    highest = lax.Precision.HIGHEST
    fs_count = lax.axis_size("fs")
    tp_count = lax.axis_size("tp")
    d_model = factors.shape[1]
    hidden_width = proj_cotangent.shape[1]
    fs_rows = d_model // fs_count
    tp_feats = saved_inputs.shape[1]
    own_rows = lax.dynamic_slice_in_dim(factors, lax.axis_index("fs") * fs_rows, fs_rows, 1).astype(
        jnp.float32
    )
    own_feats = lax.dynamic_slice_in_dim(factors, lax.axis_index("tp") * tp_feats, tp_feats, 1)
    proj_rows = jnp.dot(saved_inputs, own_feats[0], preferred_element_type=jnp.float32)
    out_rows = jnp.dot(out_cotangent, own_feats[1], preferred_element_type=jnp.float32)
    proj_rows, out_rows = lax.psum((proj_rows, out_rows), "tp")
    partial_sums = jnp.stack(
        [
            over_tokens(proj_rows, proj_cotangent.astype(jnp.float32), highest),
            over_tokens(out_rows, saved_hidden.astype(jnp.float32), highest),
        ]
    )
    small_grads = lax.psum(partial_sums, "fs")
    first_next = beta_first * moment_first + (1.0 - beta_first) * small_grads
    second_next = beta_second * moment_second + (1.0 - beta_second) * small_grads * small_grads
    direction = first_next / (jnp.sqrt(second_next) + epsilon)
    update_full = jnp.einsum("kdr,kre->kde", own_rows, direction, precision=highest)
    squares = lax.psum(jnp.sum(update_full * update_full, axis=(1, 2)), ("fs", "tp"))
    norm_scale = lax.rsqrt(squares / (d_model * hidden_width * tp_count) + epsilon)
    stepped = update_full * norm_scale[:, None, None]
    proj_next = w_proj - learn_rate * stepped[0]
    out_next = w_out - learn_rate * stepped[1].T
    proj_copy, out_copy = (
        lax.all_gather(proj_next.astype(jnp.bfloat16), "fs", axis=0, tiled=True),
        lax.all_gather(out_next.astype(jnp.bfloat16), "fs", axis=1, tiled=True),
    )
    return (proj_next, out_next, proj_copy, out_copy, first_next, second_next)


def solution(mesh):
    placed = (
        P("fs", "tp"),
        P("fs", "tp"),
        P("fs", "tp"),
        P("fs", "tp"),
        P(),
        P("fs", "tp"),
        P("tp", "fs"),
        P(None, None, "tp"),
        P(None, None, "tp"),
    )
    return jax.shard_map(
        body,
        mesh=mesh,
        in_specs=placed,
        out_specs=(
            P("fs", "tp"),
            P("tp", "fs"),
            P(None, "tp"),
            P("tp", None),
            P(None, None, "tp"),
            P(None, None, "tp"),
        ),
        check_vma=False,
    )
```

profile of v0, /device:TPU:0, one launch (start us, length us, event | category | flops | bytes accessed | tf_op | source)
XLA Modules:
  0.0 292.3 jit_solution(14841451723777137700)
XLA Ops:
  7.2 1.5 copy-done
  8.8 2.3 convolution_bitcast_fusion.1
  11.1 2.2 convolution_bitcast_fusion
  13.3 0.0 all-reduce.4.cloned.1.call-start
  13.3 60.8 %all-reduce.6.cloned.1.call-done = (f32[672,128]{0,1:T(8,128)}, f32[672,128]{0,1:T(8,128)}) async-done(((f32[672,128]{0,1:T(8,128)}, f32[672,128]{0,1:T(8,128)}), (f32[672,128]{0,1:T(8,128)}, f32[672,128]{0,1:T(8,128)})) %all-reduce.6.cloned.1.call-update) | async-done | bytes 688144 | tf_op jit(solution)/shard_map/psum | solution.py:46
  74.1 1.5 convolution_bitcast_fusion.2
  75.6 1.5 convolution_bitcast_fusion.3
  77.1 0.8 pad_maximum_fusion
  77.9 0.0 all-gather.5.cloned.1.call-start
  78.0 2.9 copy.15
  80.9 41.7 %all-reduce.4.cloned.1.call-done = f32[2,128,512]{2,1,0:T(8,128)} async-done(((f32[2,128,512]{2,1,0:T(8,128)}), f32[2,128,512]{2,1,0:T(8,128)}) %all-reduce.4.cloned.1.call-update) | async-done | bytes 524304 | tf_op jit(solution)/shard_map/psum | solution.py:53
  122.6 1.6 fusion.4
  124.2 4.0 %multiply_reduce_fusion = (f32[2]{0:T(128)S(1)}, f32[2,1024,512]{2,1,0:T(8,128)}) fusion(f32[2,128,512]{2,1,0:T(8,128)S(1)} %get-tuple-element.32, f32[2,128,512]{2,1,0:T(8,128)S(1)} %get-tuple-element.33, bf16[2,4096,128]{2,1,0:T(8,128)(2,1)S(1)} %copy-done, s32[]{:T(128)S(6)} %select_n.6), kind=kOutput, calls=%fused_computation | convolution fusion | flops 1612972032 | bytes 5767180 | tf_op jit(solution)/shard_map/kdr,kre->kde/dot_general | solution.py:57
  128.2 39.2 %psum.31 = f32[2]{0:T(128)S(1)} all-reduce(f32[2]{0:T(128)S(1)} %get-tuple-element.20), channel_id=1, replica_groups=mesh['fs'=4,'tp'=8] {'fs','tp'}, use_global_device_ids=true, to_apply=%region_4.0 | all-reduce | flops 2 | bytes 16 | tf_op jit(solution)/shard_map/psum | solution.py:58
  167.4 3.1 %broadcast_multiply_fusion = f32[2,1024,512]{2,1,0:T(8,128)S(1)} fusion(f32[2,1024,512]{2,1,0:T(8,128)} %get-tuple-element.21, f32[2]{0:T(128)S(1)} %add_rsqrt_fusion), kind=kLoop, calls=%fused_computation.7 | loop fusion | flops 1048576 | bytes 8388616 | tf_op jit(solution)/shard_map/mul | solution.py:60
  170.6 2.6 fusion.15
  173.2 0.4 copy-done.1
  173.6 0.0 all-gather.3.cloned.1.call-start
  173.6 4.5 %fusion.17 = (bf16[1024,512]{1,0:T(8,128)(2,1)}, f32[1024,512]{1,0:T(8,128)}) fusion(f32[1024,512]{1,0:T(8,128)} %param.14, f32[2,1024,512]{2,1,0:T(8,128)} %copy-done.1), kind=kLoop, calls=%fused_computation.30 | loop fusion | flops 1572864 | bytes 7340032 | tf_op jit(solution)/shard_map/convert_element_type | solution.py:64
  178.1 2.9 copy.16
  181.0 46.0 %all-gather.5.cloned.1.call-done = bf16[512,4096]{0,1:T(8,128)(2,1)} async-done(((bf16[512,1024]{0,1:T(8,128)(2,1)}), bf16[512,4096]{0,1:T(8,128)(2,1)}) %all-gather.5.cloned.1.call-update) | async-done | bytes 4194320 | tf_op jit(solution)/shard_map/all_gather | solution.py:65
  227.0 6.3 %copy.17 = bf16[512,4096]{1,0:T(8,128)(2,1)} copy(bf16[512,4096]{0,1:T(8,128)(2,1)} %all-gather.5.cloned.1.call-done) | data formatting | bytes 8388608
  233.3 48.0 %all-gather.3.cloned.1.call-done = bf16[4096,512]{1,0:T(8,128)(2,1)} async-done(((bf16[1024,512]{1,0:T(8,128)(2,1)}), bf16[4096,512]{1,0:T(8,128)(2,1)}) %all-gather.3.cloned.1.call-update) | async-done | bytes 4194320 | tf_op jit(solution)/shard_map/all_gather | solution.py:64
  281.3 4.5 %copy.22 = bf16[4096,512]{1,0:T(8,128)(2,1)} copy(bf16[4096,512]{1,0:T(8,128)(2,1)} %all-gather.3.cloned.1.call-done) | data formatting | bytes 8388608
  (18 shorter events, 0.1 us)
Async XLA Ops:
  7.2 1.6 copy-start
  7.2 66.9 %copy-start.5 = (bf16[672,512]{1,0:T(8,128)(2,1)S(1)}, bf16[672,512]{1,0:T(8,128)(2,1)}, u32[]{:S(2)}) copy-start(bf16[672,512]{1,0:T(8,128)(2,1)} %param.11) | copy-start | bytes 2064388
  7.2 66.9 %all-reduce.6.cloned.1.call-start = ((), (), s32[]{:S(2)}) async-start(), calls=%async_computation.3 | async-start | bytes 1572864 | tf_op jit(solution)/shard_map/psum | solution.py:46
  8.8 66.8 %copy-start.6 = (bf16[672,512]{1,0:T(8,128)(2,1)S(1)}, bf16[672,512]{1,0:T(8,128)(2,1)}, u32[]{:S(2)}) copy-start(bf16[672,512]{1,0:T(8,128)(2,1)} %param.10) | copy-start | bytes 2064388
  13.3 109.3 %all-reduce.4.cloned.1.call-start = ((), (), s32[]{:S(2)}) async-start(), calls=%async_computation | async-start | bytes 1048576 | tf_op jit(solution)/shard_map/psum | solution.py:53
  77.9 149.1 %all-gather.5.cloned.1.call-start = ((), (), s32[]{:S(2)}) async-start(), calls=%async_computation.2 | async-start | bytes 5242880 | tf_op jit(solution)/shard_map/all_gather | solution.py:65
  124.2 4.0 %copy-start.3 = (f32[2,128,512]{2,1,0:T(8,128)}, f32[2,128,512]{2,1,0:T(8,128)S(1)}, u32[]{:S(2)}) copy-start(f32[2,128,512]{2,1,0:T(8,128)S(1)} %get-tuple-element.33) | copy-start | bytes 1572868
  124.2 4.0 %copy-start.4 = (f32[2,128,512]{2,1,0:T(8,128)}, f32[2,128,512]{2,1,0:T(8,128)S(1)}, u32[]{:S(2)}) copy-start(f32[2,128,512]{2,1,0:T(8,128)S(1)} %get-tuple-element.32) | copy-start | bytes 1572868
  167.4 3.1 %copy-start.2 = (f32[512,1024]{0,1:T(8,128)S(1)}, f32[512,1024]{0,1:T(8,128)}, u32[]{:S(2)}) copy-start(f32[512,1024]{0,1:T(8,128)} %copy.15) | copy-start | bytes 6291460
  170.6 3.0 %copy-start.1 = (f32[2,1024,512]{2,1,0:T(8,128)}, f32[2,1024,512]{2,1,0:T(8,128)S(1)}, u32[]{:S(2)}) copy-start(f32[2,1024,512]{2,1,0:T(8,128)S(1)} %broadcast_multiply_fusion) | copy-start | bytes 12582916
  173.6 107.8 %all-gather.3.cloned.1.call-start = ((), (), s32[]{:S(2)}) async-start(), calls=%async_computation.1 | async-start | bytes 5242880 | tf_op jit(solution)/shard_map/all_gather | solution.py:64
Sparse Core Ops, SparseCore 0:
  13.4 60.6 all-reduce.5
  78.1 44.4 all-reduce.3
  173.7 53.2 all-gather.4
  228.7 52.5 all-gather.2
where the time goes:
time: 293 us; the launch traced here: 292 us
  waiting for transfers between devices  197 us (67%)
  blocking collectives  39.2 us (13%)
  local copies, waits for them, and re-layouts  18.5 us (6%)
  between operations  13.9 us (5%)
  other arithmetic  12.6 us (4%)
  matrix products  11.4 us (4%)
    psum x1, waiting for transfers between devices, body(): proj_rows, out_rows = lax.psum((proj_rows, out_rows), 'tp')  60.8 us
    all_gather x1, waiting for transfers between devices, body(): lax.all_gather(proj_next.astype(jnp.bfloat16), 'fs', axis=0, tiled=True)  48 us
    all_gather x1, waiting for transfers between devices, body(): lax.all_gather(out_next.astype(jnp.bfloat16), 'fs', axis=1, tiled=True)  46 us
    psum x1, waiting for transfers between devices, body(): small_grads = lax.psum(partial_sums, 'fs')  41.7 us
    psum x1, blocking collectives, body(): lax.psum(jnp.sum(update_full * update_full, axis=(1, 2)), ('fs', 'tp'))  39.2 us
    unnamed x18, local copies, waits for them, and re-layouts  18.5 us
  transfers between devices with their start and end apart: 4, of which 4 were waited for; matrix products, arithmetic and copies ran while one was open for 6% of the time, Pallas kernels for 0%

commit v1 on v0

--- a/solution.py
+++ b/solution.py
@@ -50,7 +50,11 @@
             over_tokens(out_rows, saved_hidden.astype(jnp.float32), highest),
         ]
     )
-    small_grads = lax.psum(partial_sums, "fs")
+    small_grads = partial_sums
+    for hop in (1, 2):
+        small_grads = small_grads + lax.ppermute(
+            small_grads, "fs", [(dev, dev ^ hop) for dev in range(4)]
+        )
     first_next = beta_first * moment_first + (1.0 - beta_first) * small_grads
     second_next = beta_second * moment_second + (1.0 - beta_second) * small_grads * small_grads
     direction = first_next / (jnp.sqrt(second_next) + epsilon)

time: 293 us -> 272 us (0.928)
  waiting for transfers between devices: 197 us -> 171 us
  starting transfers between devices: 0.16 us -> 3.2 us
    psum x1 -> x0, waiting for transfers between devices: 41.7 us -> none  [body(): small_grads = lax.psum(partial_sums, 'fs')]
    ppermute x0 -> x2, waiting for transfers between devices: none -> 17.3 us  [body(): lax.ppermute(small_grads, 'fs', [(dev, dev ^ hop) for dev in range(4)])]
    ppermute x0 -> x2, starting transfers between devices: none -> 3.08 us  [body(): lax.ppermute(small_grads, 'fs', [(dev, dev ^ hop) for dev in range(4)])]
  transfers between devices with their start and end apart: 4 -> 5, of which waited for: 4 -> 5; matrix products, arithmetic and copies ran while one was open for 6% -> 6% of each run, Pallas kernels for 0% -> 0%
where the time goes in v1:
time: 272 us; the launch traced here: 271 us
  waiting for transfers between devices  171 us (63%)
  blocking collectives  39.7 us (15%)
  local copies, waits for them, and re-layouts  19.3 us (7%)
  between operations  13.8 us (5%)
  other arithmetic  12.2 us (4%)
  matrix products  11.6 us (4%)
  starting transfers between devices  3.2 us (1%)
    psum x1, waiting for transfers between devices, body(): proj_rows, out_rows = lax.psum((proj_rows, out_rows), 'tp')  60.7 us
    all_gather x1, waiting for transfers between devices, body(): lax.all_gather(proj_next.astype(jnp.bfloat16), 'fs', axis=0, tiled=True)  48.1 us
    all_gather x1, waiting for transfers between devices, body(): lax.all_gather(out_next.astype(jnp.bfloat16), 'fs', axis=1, tiled=True)  45.2 us
    psum x1, blocking collectives, body(): lax.psum(jnp.sum(update_full * update_full, axis=(1, 2)), ('fs', 'tp'))  39.7 us
    unnamed x18, local copies, waits for them, and re-layouts  19.3 us
    ppermute x2, waiting for transfers between devices, body(): lax.ppermute(small_grads, 'fs', [(dev, dev ^ hop) for dev in range(4)])  17.3 us
  transfers between devices with their start and end apart: 5, of which 5 were waited for; matrix products, arithmetic and copies ran while one was open for 6% of the time, Pallas kernels for 0%

profile of v1, /device:TPU:0, one launch (start us, length us, event | category | flops | bytes accessed | tf_op | source)
XLA Modules:
  0.0 271.3 jit_solution(4816166301081543648)
XLA Ops:
  7.2 1.5 copy-done
  8.8 2.2 convolution_bitcast_fusion.1
  11.0 2.2 convolution_bitcast_fusion
  13.3 60.7 %all-reduce.3.cloned.1.call-done = (f32[672,128]{0,1:T(8,128)}, f32[672,128]{0,1:T(8,128)}) async-done(((f32[672,128]{0,1:T(8,128)}, f32[672,128]{0,1:T(8,128)}), (f32[672,128]{0,1:T(8,128)}, f32[672,128]{0,1:T(8,128)})) %all-reduce.3.cloned.1.call-update) | async-done | bytes 688144 | tf_op jit(solution)/shard_map/psum | solution.py:46
  74.0 1.5 convolution_bitcast_fusion.2
  75.5 1.7 convolution_bitcast_fusion.3
  77.2 1.5 collective-permute-start
  78.8 10.5 %collective-permute-done = f32[2,128,512]{2,1,0:T(8,128)S(1)} collective-permute-done((f32[2,128,512]{2,1,0:T(8,128)S(1)}, f32[2,128,512]{2,1,0:T(8,128)S(1)}, u32[]{:S(2)}, u32[]{:S(2)}) %collective-permute-start) | collective-permute-done | bytes 524320 | tf_op jit(solution)/shard_map/ppermute | solution.py:55
  89.3 0.8 copy-done.5
  90.1 1.5 collective-permute-start.1
  91.7 2.9 %copy.15 = f32[512,1024]{0,1:T(8,128)} copy(f32[512,1024]{1,0:T(8,128)} %param.15) | data formatting | bytes 4194304 | tf_op args[6]
  94.6 6.8 %collective-permute-done.1 = f32[2,128,512]{2,1,0:T(8,128)} collective-permute-done((f32[2,128,512]{2,1,0:T(8,128)S(1)}, f32[2,128,512]{2,1,0:T(8,128)}, u32[]{:S(2)}, u32[]{:S(2)}) %collective-permute-start.1) | collective-permute-done | bytes 524320 | tf_op jit(solution)/shard_map/ppermute | solution.py:55
  101.4 1.8 fusion.4
  103.3 4.0 %multiply_reduce_fusion = (f32[2]{0:T(128)S(1)}, f32[2,1024,512]{2,1,0:T(8,128)}) fusion(f32[2,128,512]{2,1,0:T(8,128)S(1)} %get-tuple-element.32, f32[2,128,512]{2,1,0:T(8,128)S(1)} %get-tuple-element.33, bf16[2,4096,128]{2,1,0:T(8,128)(2,1)S(1)} %copy-done, s32[]{:T(128)S(6)} %select_n.6), kind=kOutput, calls=%fused_computation | convolution fusion | flops 1612972032 | bytes 5767180 | tf_op jit(solution)/shard_map/kdr,kre->kde/dot_general | solution.py:61
  107.3 39.7 %psum.23 = f32[2]{0:T(128)S(1)} all-reduce(f32[2]{0:T(128)S(1)} %get-tuple-element.20), channel_id=1, replica_groups=mesh['fs'=4,'tp'=8] {'fs','tp'}, use_global_device_ids=true, to_apply=%region_3.0 | all-reduce | flops 2 | bytes 16 | tf_op jit(solution)/shard_map/psum | solution.py:62
  147.0 3.1 %broadcast_multiply_fusion = f32[2,1024,512]{2,1,0:T(8,128)S(1)} fusion(f32[2,1024,512]{2,1,0:T(8,128)} %get-tuple-element.21, f32[2]{0:T(128)S(1)} %add_rsqrt_fusion), kind=kLoop, calls=%fused_computation.7 | loop fusion | flops 1048576 | bytes 8388616 | tf_op jit(solution)/shard_map/mul | solution.py:64
  150.2 2.6 fusion.16
  152.7 0.4 copy-done.1
  153.2 4.5 %fusion.18 = (bf16[1024,512]{1,0:T(8,128)(2,1)}, f32[1024,512]{1,0:T(8,128)}) fusion(f32[1024,512]{1,0:T(8,128)} %param.14, f32[2,1024,512]{2,1,0:T(8,128)} %copy-done.1), kind=kLoop, calls=%fused_computation.31 | loop fusion | flops 1572864 | bytes 7340032 | tf_op jit(solution)/shard_map/convert_element_type | solution.py:68
  157.7 2.9 %copy.16 = f32[512,1024]{1,0:T(8,128)} copy(f32[512,1024]{0,1:T(8,128)} %get-tuple-element.15) | data formatting | bytes 4194304
  160.6 45.2 %all-gather.5.cloned.1.call-done = bf16[512,4096]{0,1:T(8,128)(2,1)} async-done(((bf16[512,1024]{0,1:T(8,128)(2,1)}), bf16[512,4096]{0,1:T(8,128)(2,1)}) %all-gather.5.cloned.1.call-update) | async-done | bytes 4194320 | tf_op jit(solution)/shard_map/all_gather | solution.py:69
  205.8 6.3 %copy.17 = bf16[512,4096]{1,0:T(8,128)(2,1)} copy(bf16[512,4096]{0,1:T(8,128)(2,1)} %all-gather.5.cloned.1.call-done) | data formatting | bytes 8388608
  212.1 48.1 %all-gather.3.cloned.1.call-done = bf16[4096,512]{1,0:T(8,128)(2,1)} async-done(((bf16[1024,512]{1,0:T(8,128)(2,1)}), bf16[4096,512]{1,0:T(8,128)(2,1)}) %all-gather.3.cloned.1.call-update) | async-done | bytes 4194320 | tf_op jit(solution)/shard_map/all_gather | solution.py:68
  260.3 4.5 %copy.21 = bf16[4096,512]{1,0:T(8,128)(2,1)} copy(bf16[4096,512]{1,0:T(8,128)(2,1)} %all-gather.3.cloned.1.call-done) | data formatting | bytes 8388608
  (20 shorter events, 0.3 us)
Async XLA Ops:
  7.2 1.6 copy-start
  7.2 66.8 %copy-start.6 = (bf16[672,512]{1,0:T(8,128)(2,1)S(1)}, bf16[672,512]{1,0:T(8,128)(2,1)}, u32[]{:S(2)}) copy-start(bf16[672,512]{1,0:T(8,128)(2,1)} %param.11) | copy-start | bytes 2064388
  7.2 66.8 %all-reduce.3.cloned.1.call-start = ((), (), s32[]{:S(2)}) async-start(), calls=%async_computation.2 | async-start | bytes 1572864 | tf_op jit(solution)/shard_map/psum | solution.py:46
  13.2 192.6 %all-gather.5.cloned.1.call-start = ((), (), s32[]{:S(2)}) async-start(), calls=%async_computation.1 | async-start | bytes 5242880 | tf_op jit(solution)/shard_map/all_gather | solution.py:69
  77.2 12.0 %collective-permute-start = (f32[2,128,512]{2,1,0:T(8,128)S(1)}, f32[2,128,512]{2,1,0:T(8,128)S(1)}, u32[]{:S(2)}, u32[]{:S(2)}) collective-permute-start(f32[2,128,512]{2,1,0:T(8,128)S(1)} %pad_maximum_fusion), channel_id=1, source_target_pairs={{0,8},{8,0},{16,24},{24,16},{1,9},{9,1},{17,25},{25,17},{2,10},{10... | collective-permute-start | bytes 1572872 | tf_op jit(solution)/shard_map/ppermute | solution.py:55
  89.3 0.8 copy-start.5
  90.1 11.3 %collective-permute-start.1 = (f32[2,128,512]{2,1,0:T(8,128)S(1)}, f32[2,128,512]{2,1,0:T(8,128)}, u32[]{:S(2)}, u32[]{:S(2)}) collective-permute-start(f32[2,128,512]{2,1,0:T(8,128)S(1)} %fusion.15), channel_id=1, source_target_pairs={{0,16},{8,24},{16,0},{24,8},{1,17},{9,25},{17,1},{25,9},{2,18},{10... | collective-permute-start | bytes 1572872 | tf_op jit(solution)/shard_map/ppermute | solution.py:55
  103.2 4.0 %copy-start.3 = (f32[2,128,512]{2,1,0:T(8,128)}, f32[2,128,512]{2,1,0:T(8,128)S(1)}, u32[]{:S(2)}) copy-start(f32[2,128,512]{2,1,0:T(8,128)S(1)} %get-tuple-element.33) | copy-start | bytes 1572868
  103.3 4.0 %copy-start.4 = (f32[2,128,512]{2,1,0:T(8,128)}, f32[2,128,512]{2,1,0:T(8,128)S(1)}, u32[]{:S(2)}) copy-start(f32[2,128,512]{2,1,0:T(8,128)S(1)} %get-tuple-element.32) | copy-start | bytes 1572868
  147.0 3.1 %copy-start.2 = (f32[512,1024]{0,1:T(8,128)S(1)}, f32[512,1024]{0,1:T(8,128)}, u32[]{:S(2)}) copy-start(f32[512,1024]{0,1:T(8,128)} %copy.15) | copy-start | bytes 6291460
  150.2 3.0 %copy-start.1 = (f32[2,1024,512]{2,1,0:T(8,128)}, f32[2,1024,512]{2,1,0:T(8,128)S(1)}, u32[]{:S(2)}) copy-start(f32[2,1024,512]{2,1,0:T(8,128)S(1)} %broadcast_multiply_fusion) | copy-start | bytes 12582916
  153.1 107.1 %all-gather.3.cloned.1.call-start = ((), (), s32[]{:S(2)}) async-start(), calls=%async_computation | async-start | bytes 5242880 | tf_op jit(solution)/shard_map/all_gather | solution.py:68
Sparse Core Ops, SparseCore 0:
  13.3 60.6 all-reduce.2
  153.3 52.4 all-gather.4
  207.7 52.5 all-gather.2
